TPU v7x, 256 devices: a whole 4x4x8 slice. The times are simulated.
256 devices in a mesh: sp: 32 (over z, x), tp: 8 (over y, core).
Axes of the slice: x: 4, y: 4, z: 8, core: 2. Of those that a mesh axis runs over, the one named last changes fastest.
Arguments:
- tokens: bfloat16 [16384, 2048], P(('sp', 'tp')), may hold values from -40 to 40
- query_weight: bfloat16 [2048, 1024], P(None, 'tp'), may hold values from -0.1875 to 0.1875
- key_weight: bfloat16 [2048, 256], replicated, may hold values from -0.1875 to 0.1875
- value_weight: bfloat16 [2048, 256], replicated, may hold values from -0.125 to 0.125
- out_weight: bfloat16 [1024, 2048], replicated, may hold values from -0.1875 to 0.1875
- head_gain: float32 [128], replicated, may hold values from 0.1 to 1.9
- lambdas: float32 [8], P('tp'), may hold values from 0.3 to 0.8
Outputs:
- mixed: bfloat16 [16384, 2048], P(('sp', 'tp'))
All inputs are finite; a program needn't handle non-finite values.
Results may differ from a plain program's by a relative error of at most 0.018.
The roundings to bfloat16 on the way count: a program that leaves them out, or rounds other values in their place, can miss the bound.
Values may be sent and summed in bfloat16 or wider, within the bound.
No kernel may reach another device: no remote copies, remote signals or barrier semaphores. Data moves between devices by JAX's collectives and lax.ppermute only.
A program may use at most 64 MiB of HBM per device.

v0:
```python
import math, functools
from jax.experimental import pallas as pl
from jax.experimental.pallas import tpu as pltpu
import jax
import jax.numpy as jnp
from jax import lax
from jax.sharding import PartitionSpec as P

DH = 64
DV = 128


epsilon = 1e-06
rope_base = 10000.0


def rotate(tensor_in, places):
    head_dim = tensor_in.shape[-1]
    half_dim = head_dim // 2
    frequency = rope_base ** (-(jnp.arange(half_dim, dtype=jnp.float32) * 2.0) / head_dim)
    angles = places[:, None] * frequency[None, :]
    angles = angles.reshape((places.shape[0],) + (1,) * (tensor_in.ndim - 2) + (half_dim,))
    cosine = jnp.cos(angles)
    sine_part = jnp.sin(angles)
    first = tensor_in[..., :half_dim]
    second = tensor_in[..., half_dim:]
    return jnp.concatenate(
        [first * cosine - second * sine_part, first * sine_part + second * cosine], axis=-1
    )


EXP_SCALE = math.log2(math.e) * 64 ** -0.5
SUM_ROW, MAX_ROW, ACC_ROWS = DV, DV + 1, DV + 8


def fold_span(q_ref, kv_ref, acc_refs, start, span, width):
    k = kv_ref[pl.ds(start, span), 0:DV]
    v = kv_ref[pl.ds(start, span), DV : 2 * DV]
    raised = jnp.concatenate([v.T, jnp.ones((ACC_ROWS - DV, span), jnp.bfloat16)], axis=0)
    per_acc = acc_refs[0].shape[1] // width
    tiles = len(acc_refs) * per_acc

    def score(j):
        q = q_ref[:, j * width : (j + 1) * width]
        return jnp.dot(k, q, preferred_element_type=jnp.float32)

    ahead = score(0)
    for j in range(tiles):
        s = ahead
        if j + 1 < tiles:
            ahead = score(j + 1)
        acc_ref = acc_refs[j // per_acc]
        cols = slice(j % per_acc * width, (j % per_acc + 1) * width)
        old = acc_ref[MAX_ROW : MAX_ROW + 1, cols]
        new = jnp.maximum(old, jnp.max(s, axis=0, keepdims=True))
        p = jnp.exp2(s * EXP_SCALE - new * EXP_SCALE).astype(jnp.bfloat16)
        shrink = jnp.exp2((old - new) * EXP_SCALE)
        added = jnp.dot(raised, p, preferred_element_type=jnp.float32)
        acc_ref[:, cols] = acc_ref[:, cols] * shrink + added
        acc_ref[MAX_ROW : MAX_ROW + 1, cols] = new


def attend_kernel(q_ref, kv_ref, *refs, span, width):
    acc_refs = refs[-2:]
    if len(refs) == 2:
        for acc_ref in acc_refs:
            acc_ref[...] = jnp.zeros(acc_ref.shape, jnp.float32)
            acc_ref[MAX_ROW : MAX_ROW + 1, :] = jnp.full((1, acc_ref.shape[1]), -3e38, jnp.float32)
    else:
        for acc_ref, old_ref in zip(acc_refs, refs):
            acc_ref[...] = old_ref[...]

    def body(i, _):
        fold_span(q_ref, kv_ref, acc_refs, pl.multiple_of(i * span, span), span, width)
        return 0

    lax.fori_loop(0, kv_ref.shape[0] // span, body, 0)


def attend(q, kv, carry=(), span=512, width=512, lim=16):
    half = q.shape[1] // 2
    vm = pl.BlockSpec(memory_space=pltpu.VMEM)
    work = kv.shape[0] * q.shape[1]
    return pl.pallas_call(
        functools.partial(attend_kernel, span=min(span, kv.shape[0]), width=width),
        out_shape=(jax.ShapeDtypeStruct((ACC_ROWS, half), jnp.float32),) * 2,
        in_specs=[vm] * (2 + len(carry)),
        out_specs=(vm, vm),
        input_output_aliases={2: 0, 3: 1} if carry else {},
        cost_estimate=pl.CostEstimate(flops=512 * work, transcendentals=work, bytes_accessed=4 * work // 1024),
        compiler_params=pltpu.CompilerParams(vmem_limit_bytes=lim * 2**20),
    )(q, kv, *carry)


def mesh_sizes():
    return lax.axis_size("sp"), lax.axis_size("tp")


X_LEN = 4


def shifted(x, dz=0, dx=0, core=0):
    sp, tp = mesh_sizes()
    pairs = []
    for s in range(sp):
        for t in range(tp):
            z = (s // X_LEN + dz) % (sp // X_LEN)
            to = z * X_LEN + (s % X_LEN + dx) % X_LEN
            pairs.append((s * tp + t, to * tp + (t ^ core)))
    return lax.ppermute(x, ("sp", "tp"), pairs)


def same_core_groups():
    tp = lax.axis_size("tp")
    return [list(range(core, tp, 2)) for core in range(2)]


def plane_groups():
    sp, tp = mesh_sizes()
    return [
        [(z * X_LEN + x) * tp + 2 * y + core for x in range(X_LEN) for y in range(tp // 2)]
        for z in range(sp // X_LEN)
        for core in range(2)
    ]


def turn(x, places):
    rows = x.shape[0]
    return rotate(x.reshape(rows, -1, DH), places).astype(jnp.bfloat16).reshape(rows, -1)


def finish_kernel(mine_ref, other_ref, lam_ref, gain_ref, out_ref):
    half = mine_ref.shape[1] // 2

    def joined(at):
        cols = slice(at, at + half)
        m1, m2 = mine_ref[MAX_ROW : MAX_ROW + 1, cols], other_ref[MAX_ROW : MAX_ROW + 1, cols]
        top = jnp.maximum(m1, m2)
        w1 = jnp.exp2((m1 - top) * EXP_SCALE)
        w2 = jnp.exp2((m2 - top) * EXP_SCALE)
        sums = slice(SUM_ROW, SUM_ROW + 1)
        total = mine_ref[sums, cols] * w1 + other_ref[sums, cols] * w2
        return (mine_ref[0:DV, cols] * w1 + other_ref[0:DV, cols] * w2) / total

    attended = joined(0) - lam_ref[0] * joined(half)
    mean_square = jnp.mean(attended * attended, axis=0, keepdims=True)
    normed = attended * lax.rsqrt(mean_square + epsilon)
    out_ref[...] = (normed.T * gain_ref[...]).astype(jnp.bfloat16)


def local(tokens, query_weight, key_weight, value_weight, out_weight, head_gain, lambdas):
    rows = tokens.shape[0]
    sp_at, tp_at = lax.axis_index("sp"), lax.axis_index("tp")
    tp = lax.axis_size("tp")
    chips = tp // 2
    core = tp_at % 2
    kv_heads = key_weight.shape[1] // (2 * DH)
    groups = same_core_groups()
    base = sp_at * (rows * tp)

    own_places = (base + tp_at * rows + jnp.arange(rows, dtype=jnp.int32)).astype(jnp.float32)
    both = jnp.concatenate([key_weight, value_weight], axis=1)
    projected = jnp.dot(tokens, both, preferred_element_type=jnp.float32)
    own_keys = turn(projected[:, : key_weight.shape[1]], own_places)
    own_values = projected[:, key_weight.shape[1] :].astype(jnp.bfloat16)
    by_group = jnp.stack(
        [
            jnp.concatenate(
                [own_keys[:, 2 * DH * g : 2 * DH * (g + 1)], own_values[:, DV * g : DV * (g + 1)]], 1
            )
            for g in range(kv_heads)
        ]
    )
    to_plane = jnp.tile(jnp.repeat(by_group, chips // kv_heads, axis=0), (X_LEN, 1, 1))
    row = lax.all_to_all(
        to_plane, ("sp", "tp"), 0, 0, axis_index_groups=plane_groups(), tiled=True
    ).reshape(-1, 2 * DH + DV)
    up = shifted(row, dz=1)
    down = shifted(row, dz=-1)

    spread = jnp.broadcast_to(tokens[None], (chips, *tokens.shape))
    near = row
    line = lax.all_to_all(spread, "tp", 0, 0, axis_index_groups=groups, tiled=True)
    line = line.reshape(chips * rows, tokens.shape[1])
    heads = jnp.concatenate([query_weight, shifted(query_weight, core=1)], axis=1)
    turned = (jnp.arange(chips, dtype=jnp.int32)[:, None] * 2 + core) * rows
    line_places = (base + turned + jnp.arange(rows, dtype=jnp.int32)[None]).reshape(-1)
    raw = jnp.dot(line, heads, preferred_element_type=jnp.float32)
    own_q = turn(raw, line_places.astype(jnp.float32))
    other_q = shifted(own_q, core=1)
    other_q = jnp.concatenate([other_q[:, 2 * DH :], other_q[:, : 2 * DH]], axis=1)
    low = jnp.where(core == 0, own_q, other_q).reshape(chips, 1, rows, 4 * DH)
    high = jnp.where(core == 0, other_q, own_q).reshape(chips, 1, rows, 4 * DH)
    queries = jnp.concatenate([low, high], axis=1).reshape(tp * rows, 4 * DH).T
    blank = jnp.zeros((DH, tp * rows), jnp.bfloat16)
    columns = jnp.concatenate(
        [
            jnp.concatenate([queries[:DH], blank, queries[2 * DH : 3 * DH], blank], 1),
            jnp.concatenate([blank, queries[DH : 2 * DH], blank, queries[3 * DH :]], 1),
        ],
        0,
    )

    half = row.shape[0] // 2
    carry = attend(columns, near)
    z_len = lax.axis_size("sp") // X_LEN
    for step in range(2, z_len // 2 + 2):
        last = step == z_len // 2
        more = step <= z_len // 2
        up, carry = lax.optimization_barrier((up, carry))
        next_up = shifted(up[:half] if last else up, dz=1) if more else None
        carry = attend(columns, up, carry)
        down, carry = lax.optimization_barrier((down, carry))
        next_down = shifted(down[half:] if last else down, dz=-1) if more else None
        carry = attend(columns, down, carry)
        up, down = next_up, next_down
    mine, other = carry
    received = shifted(other, core=1)
    vm = pl.BlockSpec(memory_space=pltpu.VMEM)
    normed = pl.pallas_call(
        finish_kernel,
        out_shape=jax.ShapeDtypeStruct((tp * rows, DV), jnp.bfloat16),
        in_specs=[vm, vm, pl.BlockSpec(memory_space=pltpu.SMEM), vm],
        out_specs=vm,
        compiler_params=pltpu.CompilerParams(vmem_limit_bytes=16 * 2**20),
    )(mine, received, lambdas, head_gain.reshape(1, DV))
    regrouped = lax.all_to_all(normed, "tp", split_axis=0, concat_axis=1, tiled=True)
    return jnp.dot(regrouped, out_weight, preferred_element_type=jnp.float32).astype(jnp.bfloat16)


def solution(mesh):
    return jax.shard_map(
        local,
        mesh=mesh,
        in_specs=(P(("sp", "tp"), None), P(None, "tp"), P(), P(), P(), P(), P("tp")),
        out_specs=P(("sp", "tp"), None),
        check_vma=False,
    )
```

profile of v0, /device:TPU:1, one launch (start us, length us, event | category | flops | bytes accessed | tf_op | source)
XLA Modules:
  0.0 103.6 jit_solution(15324459332363841636)
XLA Ops:
  0.0 2.0 %broadcast_in_dim.6 = bf16[4,64,2048]{2,1,0:T(8,128)(2,1)} broadcast(bf16[64,2048]{1,0:T(8,128)(2,1)} %param.7), dimensions={1,2} | broadcast | bytes 1310720 | tf_op jit(solution)/shard_map/broadcast_in_dim | solution.py:181
  2.0 5.1 %all-to-all-start = ((bf16[4,64,2048]{2,1,0:T(8,128)(2,1)}), bf16[4,64,2048]{2,1,0:T(8,128)(2,1)S(1)}, u32[]{:S(2)}, u32[]{:S(2)}) async-start(bf16[4,64,2048]{2,1,0:T(8,128)(2,1)} %broadcast_in_dim.6), calls=%async_computation | async-start | bytes 2097152 | tf_op jit(solution)/shard_map/all_to_all | solution.py:183
  7.2 1.8 %collective-permute-start = (bf16[2048,128]{1,0:T(8,128)(2,1)}, bf16[2048,128]{1,0:T(8,128)(2,1)S(1)}, u32[]{:S(2)}, u32[]{:S(2)}) collective-permute-start(bf16[2048,128]{1,0:T(8,128)(2,1)} %param.8), channel_id=1, source_target_pairs={{0,1},{1,0},{2,3},{3,2},{4,5},{5,4},{6,7},{7,6},{8,9},{9,8},{10,11... | collective-permute-start | bytes 1572872 | tf_op jit(solution)/shard_map/ppermute | solution.py:110
  9.0 2.1 %fusion.19 = (bf16[64,512]{1,0:T(8,128)(2,1)S(1)}, f32[64,512]{1,0:T(8,128)S(1)}) fusion(bf16[64,2048]{1,0:T(8,128)(2,1)} %param.7, bf16[2048,256]{1,0:T(8,128)(2,1)} %param.10, bf16[2048,256]{1,0:T(8,128)(2,1)} %param.9), kind=kOutput, calls=%fused_computation.40 | convolution fusion | flops 138444800 | bytes 2555904 | tf_op jit(solution)/shard_map/dot_general | solution.py:163
  12.3 8.4 %all-to-all-done = bf16[4,64,2048]{2,1,0:T(8,128)(2,1)S(1)} async-done(((bf16[4,64,2048]{2,1,0:T(8,128)(2,1)}), bf16[4,64,2048]{2,1,0:T(8,128)(2,1)S(1)}, u32[]{:S(2)}, u32[]{:S(2)}) %all-to-all-start) | async-done | bytes 1048608 | tf_op jit(solution)/shard_map/all_to_all | solution.py:183
  21.5 5.5 %all-to-all-start.1 = ((bf16[16,64,256]{2,1,0:T(8,128)(2,1)}), bf16[16,64,256]{2,1,0:T(8,128)(2,1)S(1)}, u32[]{:S(2)}, u32[]{:S(2)}) async-start(bf16[16,64,256]{2,1,0:T(8,128)(2,1)} %bitcast.13), calls=%async_computation.1 | async-start | bytes 1048576 | tf_op jit(solution)/shard_map/all_to_all | solution.py:175
  27.6 2.2 %collective-permute-start.1 = (bf16[256,256]{0,1:T(8,128)(2,1)S(1)}, bf16[256,256]{0,1:T(8,128)(2,1)S(1)}, u32[]{:S(2)}, u32[]{:S(2)}) collective-permute-start(bf16[256,256]{0,1:T(8,128)(2,1)S(1)} %bitcast.41), channel_id=1, source_target_pairs={{0,1},{1,0},{2,3},{3,2},{4,5},{5,4},{6,7},{7,6},{8,9},{9,8},{10,11... | collective-permute-start | bytes 393224 | tf_op jit(solution)/shard_map/ppermute | solution.py:110
  29.8 6.4 %all-to-all-done.1 = bf16[16,64,256]{2,1,0:T(8,128)(2,1)S(1)} async-done(((bf16[16,64,256]{2,1,0:T(8,128)(2,1)}), bf16[16,64,256]{2,1,0:T(8,128)(2,1)S(1)}, u32[]{:S(2)}, u32[]{:S(2)}) %all-to-all-start.1) | async-done | bytes 524320 | tf_op jit(solution)/shard_map/all_to_all | solution.py:175
  36.2 1.6 %collective-permute-start.3 = (bf16[1024,256]{1,0:T(8,128)(2,1)S(1)}, bf16[1024,256]{1,0:T(8,128)(2,1)S(1)}, u32[]{:S(2)}, u32[]{:S(2)}) collective-permute-start(bf16[1024,256]{1,0:T(8,128)(2,1)S(1)} %bitcast.33), channel_id=1, source_target_pairs={{0,32},{1,33},{2,34},{3,35},{4,36},{5,37},{6,38},{7,39},{8,40},{9,... | collective-permute-start | bytes 1572872 | tf_op jit(solution)/shard_map/ppermute | solution.py:110
  37.8 3.9 %collective-permute-start.2 = (bf16[1024,256]{1,0:T(8,128)(2,1)S(1)}, bf16[1024,256]{1,0:T(8,128)(2,1)S(1)}, u32[]{:S(2)}, u32[]{:S(2)}) collective-permute-start(bf16[1024,256]{1,0:T(8,128)(2,1)S(1)} %bitcast.34), channel_id=1, source_target_pairs={{0,224},{1,225},{2,226},{3,227},{4,228},{5,229},{6,230},{7,231},{8... | collective-permute-start | bytes 1572872 | tf_op jit(solution)/shard_map/ppermute | solution.py:110
  42.8 3.2 %shard_map.73 = (f32[136,1024]{1,0:T(8,128)S(1)}, f32[136,1024]{1,0:T(8,128)S(1)}) custom-call(bf16[128,2048]{1,0:T(8,128)(2,1)S(1)} %maximum_maximum_fusion.q_ref, bf16[1024,256]{1,0:T(8,128)(2,1)S(1)} %bitcast.35), custom_call_target="tpu_custom_call" | custom-call | flops 1073741824 | bytes 8192 | tf_op jit(solution)/shard_map/pallas_call | solution.py:84
  46.0 4.8 %collective-permute-done.3.kv_ref = bf16[1024,256]{1,0:T(8,128)(2,1)S(1)} collective-permute-done((bf16[1024,256]{1,0:T(8,128)(2,1)S(1)}, bf16[1024,256]{1,0:T(8,128)(2,1)S(1)}, u32[]{:S(2)}, u32[]{:S(2)}) %collective-permute-start.3) | collective-permute-done | bytes 524320 | tf_op jit(solution)/shard_map/ppermute | solution.py:110
  50.8 3.3 %shard_map.74 = (f32[136,1024]{1,0:T(8,128)S(1)}, f32[136,1024]{1,0:T(8,128)S(1)}) custom-call(bf16[128,2048]{1,0:T(8,128)(2,1)S(1)} %maximum_maximum_fusion.q_ref, bf16[1024,256]{1,0:T(8,128)(2,1)S(1)} %collective-permute-done.3.kv_ref, f32[136,1024]{1,0:T(8,128)S(1)} %get-tuple-element.50.refs_0_, ...), custom_call_target="tpu_custom_call", output_to_operand_aliasing={{0}: (2, {}), {1}: (3, {})} | custom-call | flops 1073741824 | bytes 8192 | tf_op jit(solution)/shard_map/pallas_call | solution.py:84
  54.2 2.7 %collective-permute-start.4 = (bf16[1024,256]{1,0:T(8,128)(2,1)S(1)}, bf16[1024,256]{1,0:T(8,128)(2,1)S(1)}, u32[]{:S(2)}, u32[]{:S(2)}) collective-permute-start(bf16[1024,256]{1,0:T(8,128)(2,1)S(1)} %collective-permute-done.2.kv_ref), channel_id=1, source_target_pairs={{0,224},{1,225},{2,226},{3,227},{4,228},{5,229},{6,230},{7,231},{8... | collective-permute-start | bytes 1572872 | tf_op jit(solution)/shard_map/ppermute | solution.py:110
  56.9 3.3 %shard_map.75 = (f32[136,1024]{1,0:T(8,128)S(1)}, f32[136,1024]{1,0:T(8,128)S(1)}) custom-call(bf16[128,2048]{1,0:T(8,128)(2,1)S(1)} %maximum_maximum_fusion.q_ref, bf16[1024,256]{1,0:T(8,128)(2,1)S(1)} %collective-permute-done.2.kv_ref, f32[136,1024]{1,0:T(8,128)S(1)} %get-tuple-element.55.refs_0_, ...), custom_call_target="tpu_custom_call", output_to_operand_aliasing={{0}: (2, {}), {1}: (3, {})} | custom-call | flops 1073741824 | bytes 8192 | tf_op jit(solution)/shard_map/pallas_call | solution.py:84
  61.7 3.3 %shard_map.76 = (f32[136,1024]{1,0:T(8,128)S(1)}, f32[136,1024]{1,0:T(8,128)S(1)}) custom-call(bf16[128,2048]{1,0:T(8,128)(2,1)S(1)} %maximum_maximum_fusion.q_ref, bf16[1024,256]{1,0:T(8,128)(2,1)S(1)} %collective-permute-done.5.kv_ref, f32[136,1024]{1,0:T(8,128)S(1)} %get-tuple-element.60.refs_0_, ...), custom_call_target="tpu_custom_call", output_to_operand_aliasing={{0}: (2, {}), {1}: (3, {})} | custom-call | flops 1073741824 | bytes 8192 | tf_op jit(solution)/shard_map/pallas_call | solution.py:84
  65.0 2.7 %collective-permute-start.6 = (bf16[1024,256]{1,0:T(8,128)(2,1)S(1)}, bf16[1024,256]{1,0:T(8,128)(2,1)S(1)}, u32[]{:S(2)}, u32[]{:S(2)}) collective-permute-start(bf16[1024,256]{1,0:T(8,128)(2,1)S(1)} %collective-permute-done.4.kv_ref), channel_id=1, source_target_pairs={{0,224},{1,225},{2,226},{3,227},{4,228},{5,229},{6,230},{7,231},{8... | collective-permute-start | bytes 1572872 | tf_op jit(solution)/shard_map/ppermute | solution.py:110
  67.8 3.3 %shard_map.77 = (f32[136,1024]{1,0:T(8,128)S(1)}, f32[136,1024]{1,0:T(8,128)S(1)}) custom-call(bf16[128,2048]{1,0:T(8,128)(2,1)S(1)} %maximum_maximum_fusion.q_ref, bf16[1024,256]{1,0:T(8,128)(2,1)S(1)} %collective-permute-done.4.kv_ref, f32[136,1024]{1,0:T(8,128)S(1)} %get-tuple-element.65.refs_0_, ...), custom_call_target="tpu_custom_call", output_to_operand_aliasing={{0}: (2, {}), {1}: (3, {})} | custom-call | flops 1073741824 | bytes 8192 | tf_op jit(solution)/shard_map/pallas_call | solution.py:84
  72.2 3.3 %shard_map.78 = (f32[136,1024]{1,0:T(8,128)S(1)}, f32[136,1024]{1,0:T(8,128)S(1)}) custom-call(bf16[128,2048]{1,0:T(8,128)(2,1)S(1)} %maximum_maximum_fusion.q_ref, bf16[1024,256]{1,0:T(8,128)(2,1)S(1)} %collective-permute-done.7.kv_ref, f32[136,1024]{1,0:T(8,128)S(1)} %get-tuple-element.70.refs_0_, ...), custom_call_target="tpu_custom_call", output_to_operand_aliasing={{0}: (2, {}), {1}: (3, {})} | custom-call | flops 1073741824 | bytes 8192 | tf_op jit(solution)/shard_map/pallas_call | solution.py:84
  75.6 2.7 %collective-permute-start.8 = (bf16[512,256]{1,0:T(8,128)(2,1)S(1)}, bf16[512,256]{1,0:T(8,128)(2,1)S(1)}, u32[]{:S(2)}, u32[]{:S(2)}) collective-permute-start(bf16[512,256]{1,0:T(8,128)(2,1)S(1)} %slice.70), channel_id=1, source_target_pairs={{0,224},{1,225},{2,226},{3,227},{4,228},{5,229},{6,230},{7,231},{8... | collective-permute-start | bytes 786440 | tf_op jit(solution)/shard_map/ppermute | solution.py:110
  78.3 3.3 %shard_map.79 = (f32[136,1024]{1,0:T(8,128)S(1)}, f32[136,1024]{1,0:T(8,128)S(1)}) custom-call(bf16[128,2048]{1,0:T(8,128)(2,1)S(1)} %maximum_maximum_fusion.q_ref, bf16[1024,256]{1,0:T(8,128)(2,1)S(1)} %collective-permute-done.6.kv_ref, f32[136,1024]{1,0:T(8,128)S(1)} %get-tuple-element.75.refs_0_, ...), custom_call_target="tpu_custom_call", output_to_operand_aliasing={{0}: (2, {}), {1}: (3, {})} | custom-call | flops 1073741824 | bytes 8192 | tf_op jit(solution)/shard_map/pallas_call | solution.py:84
  83.3 1.6 %shard_map.81 = (f32[136,1024]{1,0:T(8,128)S(1)}, f32[136,1024]{1,0:T(8,128)S(1)}) custom-call(bf16[128,2048]{1,0:T(8,128)(2,1)S(1)} %maximum_maximum_fusion.q_ref, bf16[512,256]{1,0:T(8,128)(2,1)S(1)} %collective-permute-done.8.kv_ref, f32[136,1024]{1,0:T(8,128)S(1)} %get-tuple-element.85.refs_0_, ...), custom_call_target="tpu_custom_call", output_to_operand_aliasing={{0}: (2, {}), {1}: (3, {})} | custom-call | flops 536870912 | bytes 4096 | tf_op jit(solution)/shard_map/pallas_call | solution.py:84
  84.9 7.3 %collective-permute-start.10 = (f32[136,1024]{1,0:T(8,128)S(1)}, f32[136,1024]{1,0:T(8,128)S(1)}, u32[]{:S(2)}, u32[]{:S(2)}) collective-permute-start(f32[136,1024]{1,0:T(8,128)S(1)} %get-tuple-element.88), channel_id=1, source_target_pairs={{0,1},{1,0},{2,3},{3,2},{4,5},{5,4},{6,7},{7,6},{8,9},{9,8},{10,11... | collective-permute-start | bytes 1671176 | tf_op jit(solution)/shard_map/ppermute | solution.py:110
  94.1 8.0 %all_to_all.29 = bf16[8,64,128]{2,1,0:T(8,128)(2,1)S(1)} all-to-all(bf16[8,64,128]{2,1,0:T(8,128)(2,1)S(1)} %bitcast.36), channel_id=1, replica_groups=mesh['sp'=32,'tp'=8] {'tp'}, dimensions={0} | all-to-all | bytes 262144 | tf_op jit(solution)/shard_map/all_to_all | solution.py:227
  (57 shorter events, 10.4 us)
Async XLA Ops:
  2.0 25.0 %copy-start.2 = (bf16[2048,128]{1,0:T(8,128)(2,1)S(1)}, bf16[2048,128]{1,0:T(8,128)(2,1)}, u32[]{:S(2)}) copy-start(bf16[2048,128]{1,0:T(8,128)(2,1)} %param.8) | copy-start | bytes 1572868
  2.0 18.6 %all-to-all-start = ((bf16[4,64,2048]{2,1,0:T(8,128)(2,1)}), bf16[4,64,2048]{2,1,0:T(8,128)(2,1)S(1)}, u32[]{:S(2)}, u32[]{:S(2)}) async-start(bf16[4,64,2048]{2,1,0:T(8,128)(2,1)} %broadcast_in_dim.6), calls=%async_computation | async-start | bytes 2097152 | tf_op jit(solution)/shard_map/all_to_all | solution.py:183
  7.2 19.8 %collective-permute-start = (bf16[2048,128]{1,0:T(8,128)(2,1)}, bf16[2048,128]{1,0:T(8,128)(2,1)S(1)}, u32[]{:S(2)}, u32[]{:S(2)}) collective-permute-start(bf16[2048,128]{1,0:T(8,128)(2,1)} %param.8), channel_id=1, source_target_pairs={{0,1},{1,0},{2,3},{3,2},{4,5},{5,4},{6,7},{7,6},{8,9},{9,8},{10,11... | collective-permute-start | bytes 1572872 | tf_op jit(solution)/shard_map/ppermute | solution.py:110
  21.5 14.7 %all-to-all-start.1 = ((bf16[16,64,256]{2,1,0:T(8,128)(2,1)}), bf16[16,64,256]{2,1,0:T(8,128)(2,1)S(1)}, u32[]{:S(2)}, u32[]{:S(2)}) async-start(bf16[16,64,256]{2,1,0:T(8,128)(2,1)} %bitcast.13), calls=%async_computation.1 | async-start | bytes 1048576 | tf_op jit(solution)/shard_map/all_to_all | solution.py:175
  27.6 14.5 %collective-permute-start.1 = (bf16[256,256]{0,1:T(8,128)(2,1)S(1)}, bf16[256,256]{0,1:T(8,128)(2,1)S(1)}, u32[]{:S(2)}, u32[]{:S(2)}) collective-permute-start(bf16[256,256]{0,1:T(8,128)(2,1)S(1)} %bitcast.41), channel_id=1, source_target_pairs={{0,1},{1,0},{2,3},{3,2},{4,5},{5,4},{6,7},{7,6},{8,9},{9,8},{10,11... | collective-permute-start | bytes 393224 | tf_op jit(solution)/shard_map/ppermute | solution.py:110
  36.2 14.6 %collective-permute-start.3 = (bf16[1024,256]{1,0:T(8,128)(2,1)S(1)}, bf16[1024,256]{1,0:T(8,128)(2,1)S(1)}, u32[]{:S(2)}, u32[]{:S(2)}) collective-permute-start(bf16[1024,256]{1,0:T(8,128)(2,1)S(1)} %bitcast.33), channel_id=1, source_target_pairs={{0,32},{1,33},{2,34},{3,35},{4,36},{5,37},{6,38},{7,39},{8,40},{9,... | collective-permute-start | bytes 1572872 | tf_op jit(solution)/shard_map/ppermute | solution.py:110
  37.8 16.3 %collective-permute-start.2 = (bf16[1024,256]{1,0:T(8,128)(2,1)S(1)}, bf16[1024,256]{1,0:T(8,128)(2,1)S(1)}, u32[]{:S(2)}, u32[]{:S(2)}) collective-permute-start(bf16[1024,256]{1,0:T(8,128)(2,1)S(1)} %bitcast.34), channel_id=1, source_target_pairs={{0,224},{1,225},{2,226},{3,227},{4,228},{5,229},{6,230},{7,231},{8... | collective-permute-start | bytes 1572872 | tf_op jit(solution)/shard_map/ppermute | solution.py:110
  50.8 10.9 %collective-permute-start.5 = (bf16[1024,256]{1,0:T(8,128)(2,1)S(1)}, bf16[1024,256]{1,0:T(8,128)(2,1)S(1)}, u32[]{:S(2)}, u32[]{:S(2)}) collective-permute-start(bf16[1024,256]{1,0:T(8,128)(2,1)S(1)} %collective-permute-done.3.kv_ref), channel_id=1, source_target_pairs={{0,32},{1,33},{2,34},{3,35},{4,36},{5,37},{6,38},{7,39},{8,40},{9,... | collective-permute-start | bytes 1572872 | tf_op jit(solution)/shard_map/ppermute | solution.py:110
  54.2 10.9 %collective-permute-start.4 = (bf16[1024,256]{1,0:T(8,128)(2,1)S(1)}, bf16[1024,256]{1,0:T(8,128)(2,1)S(1)}, u32[]{:S(2)}, u32[]{:S(2)}) collective-permute-start(bf16[1024,256]{1,0:T(8,128)(2,1)S(1)} %collective-permute-done.2.kv_ref), channel_id=1, source_target_pairs={{0,224},{1,225},{2,226},{3,227},{4,228},{5,229},{6,230},{7,231},{8... | collective-permute-start | bytes 1572872 | tf_op jit(solution)/shard_map/ppermute | solution.py:110
  61.7 10.4 %collective-permute-start.7 = (bf16[1024,256]{1,0:T(8,128)(2,1)S(1)}, bf16[1024,256]{1,0:T(8,128)(2,1)S(1)}, u32[]{:S(2)}, u32[]{:S(2)}) collective-permute-start(bf16[1024,256]{1,0:T(8,128)(2,1)S(1)} %collective-permute-done.5.kv_ref), channel_id=1, source_target_pairs={{0,32},{1,33},{2,34},{3,35},{4,36},{5,37},{6,38},{7,39},{8,40},{9,... | collective-permute-start | bytes 1572872 | tf_op jit(solution)/shard_map/ppermute | solution.py:110
  65.0 10.5 %collective-permute-start.6 = (bf16[1024,256]{1,0:T(8,128)(2,1)S(1)}, bf16[1024,256]{1,0:T(8,128)(2,1)S(1)}, u32[]{:S(2)}, u32[]{:S(2)}) collective-permute-start(bf16[1024,256]{1,0:T(8,128)(2,1)S(1)} %collective-permute-done.4.kv_ref), channel_id=1, source_target_pairs={{0,224},{1,225},{2,226},{3,227},{4,228},{5,229},{6,230},{7,231},{8... | collective-permute-start | bytes 1572872 | tf_op jit(solution)/shard_map/ppermute | solution.py:110
  72.1 9.5 %collective-permute-start.9 = (bf16[512,256]{1,0:T(8,128)(2,1)S(1)}, bf16[512,256]{1,0:T(8,128)(2,1)S(1)}, u32[]{:S(2)}, u32[]{:S(2)}) collective-permute-start(bf16[512,256]{1,0:T(8,128)(2,1)S(1)} %slice.71), channel_id=1, source_target_pairs={{0,32},{1,33},{2,34},{3,35},{4,36},{5,37},{6,38},{7,39},{8,40},{9,... | collective-permute-start | bytes 786440 | tf_op jit(solution)/shard_map/ppermute | solution.py:110
  75.5 18.2 %copy-start = (f32[128]{0:T(128)S(1)}, f32[128]{0:T(128)}, u32[]{:S(2)}) copy-start(f32[128]{0:T(128)} %param.12) | copy-start | bytes 1540
  75.6 26.5 %copy-start.1 = (bf16[1024,2048]{1,0:T(8,128)(2,1)S(1)}, bf16[1024,2048]{1,0:T(8,128)(2,1)}, u32[]{:S(2)}) copy-start(bf16[1024,2048]{1,0:T(8,128)(2,1)} %param.11) | copy-start | bytes 12582916
  75.6 7.7 %collective-permute-start.8 = (bf16[512,256]{1,0:T(8,128)(2,1)S(1)}, bf16[512,256]{1,0:T(8,128)(2,1)S(1)}, u32[]{:S(2)}, u32[]{:S(2)}) collective-permute-start(bf16[512,256]{1,0:T(8,128)(2,1)S(1)} %slice.70), channel_id=1, source_target_pairs={{0,224},{1,225},{2,226},{3,227},{4,228},{5,229},{6,230},{7,231},{8... | collective-permute-start | bytes 786440 | tf_op jit(solution)/shard_map/ppermute | solution.py:110
  84.9 8.9 %collective-permute-start.10 = (f32[136,1024]{1,0:T(8,128)S(1)}, f32[136,1024]{1,0:T(8,128)S(1)}, u32[]{:S(2)}, u32[]{:S(2)}) collective-permute-start(f32[136,1024]{1,0:T(8,128)S(1)} %get-tuple-element.88), channel_id=1, source_target_pairs={{0,1},{1,0},{2,3},{3,2},{4,5},{5,4},{6,7},{7,6},{8,9},{9,8},{10,11... | collective-permute-start | bytes 1671176 | tf_op jit(solution)/shard_map/ppermute | solution.py:110
where the time goes:
time: 104 us
  starting transfers between devices  35.8 us (34%)
  Pallas kernels  26.6 us (26%)
  waiting for transfers between devices  23.1 us (22%)
  blocking collectives  8 us (8%)
  matrix products  4.13 us (4%)
  local copies, waits for them, and re-layouts  4.02 us (4%)
    pallas_call x9, Pallas kernels, attend(): pl.pallas_call(functools.partial(attend_kernel, span=min(span, kv.shape[0...  26.3 us
    ppermute x11, starting transfers between devices, shifted(): return lax.ppermute(x, ('sp', 'tp'), pairs)  25.2 us
    all_to_all x1, waiting for transfers between devices, local(): lax.all_to_all(spread, 'tp', 0, 0, axis_index_groups=groups, tiled=True)  8.39 us
    ppermute x11, waiting for transfers between devices, shifted(): return lax.ppermute(x, ('sp', 'tp'), pairs)  8.24 us
    all_to_all x1, blocking collectives, local(): lax.all_to_all(normed, 'tp', split_axis=0, concat_axis=1, tiled=True)  8 us
    all_to_all x1, waiting for transfers between devices, local(): lax.all_to_all(to_plane, ('sp', 'tp'), 0, 0, axis_index_groups=plane_grou...  6.44 us
    all_to_all x1, starting transfers between devices, local(): lax.all_to_all(to_plane, ('sp', 'tp'), 0, 0, axis_index_groups=plane_grou...  5.46 us
    all_to_all x1, starting transfers between devices, local(): lax.all_to_all(spread, 'tp', 0, 0, axis_index_groups=groups, tiled=True)  5.13 us
  transfers between devices with their start and end apart: 13, of which 6 were waited for; matrix products, arithmetic and copies ran while one was open for 5% of the time, Pallas kernels for 24%

commit v1 on v0

--- a/solution.py
+++ b/solution.py
@@ -99,20 +99,14 @@
 X_LEN = 4
 
 
-def shifted(x, dz=0, dx=0, core=0):
+def shifted(x, dz=0, dy=0, core=0):
     sp, tp = mesh_sizes()
     pairs = []
     for s in range(sp):
         for t in range(tp):
-            z = (s // X_LEN + dz) % (sp // X_LEN)
-            to = z * X_LEN + (s % X_LEN + dx) % X_LEN
-            pairs.append((s * tp + t, to * tp + (t ^ core)))
+            to = (s + dz * X_LEN) % sp
+            pairs.append((s * tp + t, to * tp + (t + 2 * dy) % tp ^ core))
     return lax.ppermute(x, ("sp", "tp"), pairs)
-
-
-def same_core_groups():
-    tp = lax.axis_size("tp")
-    return [list(range(core, tp, 2)) for core in range(2)]
 
 
 def plane_groups():
@@ -155,7 +149,6 @@
     chips = tp // 2
     core = tp_at % 2
     kv_heads = key_weight.shape[1] // (2 * DH)
-    groups = same_core_groups()
     base = sp_at * (rows * tp)
 
     own_places = (base + tp_at * rows + jnp.arange(rows, dtype=jnp.int32)).astype(jnp.float32)
@@ -178,14 +171,20 @@
     up = shifted(row, dz=1)
     down = shifted(row, dz=-1)
 
-    spread = jnp.broadcast_to(tokens[None], (chips, *tokens.shape))
     near = row
-    line = lax.all_to_all(spread, "tp", 0, 0, axis_index_groups=groups, tiled=True)
-    line = line.reshape(chips * rows, tokens.shape[1])
+    pieces = [tokens]
+    for d in range(1, chips):
+        pieces.append(shifted(tokens, dy=d))
     heads = jnp.concatenate([query_weight, shifted(query_weight, core=1)], axis=1)
+    raw = jnp.concatenate(
+        [jnp.dot(p, heads, preferred_element_type=jnp.float32) for p in pieces[::-1]], axis=0
+    )
+    at = tp_at // 2
+    raw = lax.dynamic_slice_in_dim(
+        jnp.concatenate([raw, raw[: (chips - 1) * rows]]), (chips - 1 - at) * rows, chips * rows, 0
+    )
     turned = (jnp.arange(chips, dtype=jnp.int32)[:, None] * 2 + core) * rows
     line_places = (base + turned + jnp.arange(rows, dtype=jnp.int32)[None]).reshape(-1)
-    raw = jnp.dot(line, heads, preferred_element_type=jnp.float32)
     own_q = turn(raw, line_places.astype(jnp.float32))
     other_q = shifted(own_q, core=1)
     other_q = jnp.concatenate([other_q[:, 2 * DH :], other_q[:, : 2 * DH]], axis=1)
@@ -207,10 +206,12 @@
     for step in range(2, z_len // 2 + 2):
         last = step == z_len // 2
         more = step <= z_len // 2
-        up, carry = lax.optimization_barrier((up, carry))
+        if step > 2:
+            up, carry = lax.optimization_barrier((up, carry))
         next_up = shifted(up[:half] if last else up, dz=1) if more else None
         carry = attend(columns, up, carry)
-        down, carry = lax.optimization_barrier((down, carry))
+        if step > 2:
+            down, carry = lax.optimization_barrier((down, carry))
         next_down = shifted(down[half:] if last else down, dz=-1) if more else None
         carry = attend(columns, down, carry)
         up, down = next_up, next_down

time: 104 us -> 97 us (0.933)
  waiting for transfers between devices: 23.1 us -> 18.5 us
  starting transfers between devices: 35.8 us -> 31.6 us
  blocking collectives: 8 us -> 9.94 us
  local copies, waits for them, and re-layouts: 4.02 us -> 2.24 us
  matrix products: 4.13 us -> 5.78 us
    all_to_all x1 -> x0, waiting for transfers between devices: 8.39 us -> none  [local(): lax.all_to_all(spread, 'tp', 0, 0, axis_index_groups=groups, tiled=True)]
    all_to_all x1 -> x0, starting transfers between devices: 5.13 us -> none  [local(): lax.all_to_all(spread, 'tp', 0, 0, axis_index_groups=groups, tiled=True)]
    ppermute x11 -> x14, waiting for transfers between devices: 8.24 us -> 13.3 us  [shifted(): return lax.ppermute(x, ('sp', 'tp'), pairs)]
    broadcast_in_dim x1 -> x0, local copies, waits for them, and re-layouts: 2.04 us -> none  [local(): spread = jnp.broadcast_to(tokens[None], (chips, *tokens.shape))]
    all_to_all x1, blocking collectives: 8 us -> 9.94 us  [local(): lax.all_to_all(normed, 'tp', split_axis=0, concat_axis=1, tiled=True)]
    dot_general x1 -> x4, matrix products: 0.48 us -> 2.13 us  [local(): jnp.dot(p, heads, preferred_element_type=jnp.float32)]
    all_to_all x1, waiting for transfers between devices: 6.44 us -> 5.18 us  [local(): lax.all_to_all(to_plane, ('sp', 'tp'), 0, 0, axis_index_groups=plane_grou...]
    ppermute x11 -> x14, starting transfers between devices: 25.2 us -> 25.8 us  [shifted(): return lax.ppermute(x, ('sp', 'tp'), pairs)]
  transfers between devices with their start and end apart: 13 -> 15, of which waited for: 6 -> 5; matrix products, arithmetic and copies ran while one was open for 5% -> 8% of each run, Pallas kernels for 24% -> 26%
where the time goes in v1:
time: 97 us; the launch traced here: 96.8 us
  starting transfers between devices  31.6 us (33%)
  Pallas kernels  26.6 us (27%)
  waiting for transfers between devices  18.5 us (19%)
  blocking collectives  9.94 us (10%)
  matrix products  5.78 us (6%)
  local copies, waits for them, and re-layouts  2.24 us (2%)
  between operations  1.15 us (1%)
  other arithmetic  0.97 us (1%)
    pallas_call x9, Pallas kernels, attend(): pl.pallas_call(functools.partial(attend_kernel, span=min(span, kv.shape[0...  26.3 us
    ppermute x14, starting transfers between devices, shifted(): return lax.ppermute(x, ('sp', 'tp'), pairs)  25.8 us
    ppermute x14, waiting for transfers between devices, shifted(): return lax.ppermute(x, ('sp', 'tp'), pairs)  13.3 us
    all_to_all x1, blocking collectives, local(): lax.all_to_all(normed, 'tp', split_axis=0, concat_axis=1, tiled=True)  9.94 us
    all_to_all x1, starting transfers between devices, local(): lax.all_to_all(to_plane, ('sp', 'tp'), 0, 0, axis_index_groups=plane_grou...  5.83 us
    all_to_all x1, waiting for transfers between devices, local(): lax.all_to_all(to_plane, ('sp', 'tp'), 0, 0, axis_index_groups=plane_grou...  5.18 us
    dot_general x4, matrix products, local(): jnp.dot(p, heads, preferred_element_type=jnp.float32)  2.13 us
    dot_general x1, matrix products, local(): projected = jnp.dot(tokens, both, preferred_element_type=jnp.float32)  2.11 us
  transfers between devices with their start and end apart: 15, of which 5 were waited for; matrix products, arithmetic and copies ran while one was open for 8% of the time, Pallas kernels for 26%

profile of v1, /device:TPU:1, one launch (start us, length us, event | category | flops | bytes accessed | tf_op | source)
XLA Modules:
  0.0 96.8 jit_solution(18112610380602142145)
XLA Ops:
  0.0 3.6 %collective-permute-start.1 = (bf16[64,2048]{1,0:T(8,128)(2,1)}, bf16[64,2048]{1,0:T(8,128)(2,1)}, u32[]{:S(2)}, u32[]{:S(2)}) collective-permute-start(bf16[64,2048]{1,0:T(8,128)(2,1)} %param.7), channel_id=1, source_target_pairs={{0,6},{1,7},{2,0},{3,1},{4,2},{5,3},{6,4},{7,5},{8,14},{9,15},{10,... | collective-permute-start | bytes 786440 | tf_op jit(solution)/shard_map/ppermute | solution.py:109
  4.6 1.5 %collective-permute-start = (bf16[2048,128]{1,0:T(8,128)(2,1)}, bf16[2048,128]{1,0:T(8,128)(2,1)S(1)}, u32[]{:S(2)}, u32[]{:S(2)}) collective-permute-start(bf16[2048,128]{1,0:T(8,128)(2,1)} %param.8), channel_id=1, source_target_pairs={{0,1},{1,0},{2,3},{3,2},{4,5},{5,4},{6,7},{7,6},{8,9},{9,8},{10,11... | collective-permute-start | bytes 1572872 | tf_op jit(solution)/shard_map/ppermute | solution.py:109
  6.1 2.1 %fusion.15 = (bf16[64,512]{1,0:T(8,128)(2,1)S(1)}, f32[64,512]{1,0:T(8,128)S(1)}) fusion(bf16[64,2048]{1,0:T(8,128)(2,1)} %param.7, bf16[2048,256]{1,0:T(8,128)(2,1)} %param.10, bf16[2048,256]{1,0:T(8,128)(2,1)} %param.9), kind=kOutput, calls=%fused_computation.49 | convolution fusion | flops 138444800 | bytes 2555904 | tf_op jit(solution)/shard_map/dot_general | solution.py:156
  9.9 5.8 %all-to-all-start = ((bf16[16,64,256]{2,1,0:T(8,128)(2,1)}), bf16[16,64,256]{2,1,0:T(8,128)(2,1)S(1)}, u32[]{:S(2)}, u32[]{:S(2)}) async-start(bf16[16,64,256]{2,1,0:T(8,128)(2,1)} %bitcast.14), calls=%async_computation | async-start | bytes 1048576 | tf_op jit(solution)/shard_map/all_to_all | solution.py:168
  20.7 5.2 %all-to-all-done = bf16[16,64,256]{2,1,0:T(8,128)(2,1)S(1)} async-done(((bf16[16,64,256]{2,1,0:T(8,128)(2,1)}), bf16[16,64,256]{2,1,0:T(8,128)(2,1)S(1)}, u32[]{:S(2)}, u32[]{:S(2)}) %all-to-all-start) | async-done | bytes 524320 | tf_op jit(solution)/shard_map/all_to_all | solution.py:168
  25.9 1.6 %collective-permute-start.7 = (bf16[1024,256]{1,0:T(8,128)(2,1)S(1)}, bf16[1024,256]{1,0:T(8,128)(2,1)S(1)}, u32[]{:S(2)}, u32[]{:S(2)}) collective-permute-start(bf16[1024,256]{1,0:T(8,128)(2,1)S(1)} %bitcast.47), channel_id=1, source_target_pairs={{0,32},{1,33},{2,34},{3,35},{4,36},{5,37},{6,38},{7,39},{8,40},{9,... | collective-permute-start | bytes 1572872 | tf_op jit(solution)/shard_map/ppermute | solution.py:109
  27.5 3.9 %collective-permute-start.5 = (bf16[1024,256]{1,0:T(8,128)(2,1)S(1)}, bf16[1024,256]{1,0:T(8,128)(2,1)S(1)}, u32[]{:S(2)}, u32[]{:S(2)}) collective-permute-start(bf16[1024,256]{1,0:T(8,128)(2,1)S(1)} %bitcast.48), channel_id=1, source_target_pairs={{0,224},{1,225},{2,226},{3,227},{4,228},{5,229},{6,230},{7,231},{8... | collective-permute-start | bytes 1572872 | tf_op jit(solution)/shard_map/ppermute | solution.py:109
  32.1 9.3 %collective-permute-done.7.kv_ref = bf16[1024,256]{1,0:T(8,128)(2,1)S(1)} collective-permute-done((bf16[1024,256]{1,0:T(8,128)(2,1)S(1)}, bf16[1024,256]{1,0:T(8,128)(2,1)S(1)}, u32[]{:S(2)}, u32[]{:S(2)}) %collective-permute-start.7) | collective-permute-done | bytes 524320 | tf_op jit(solution)/shard_map/ppermute | solution.py:109
  41.4 2.7 %collective-permute-start.6 = (bf16[1024,256]{1,0:T(8,128)(2,1)S(1)}, bf16[1024,256]{1,0:T(8,128)(2,1)S(1)}, u32[]{:S(2)}, u32[]{:S(2)}) collective-permute-start(bf16[1024,256]{1,0:T(8,128)(2,1)S(1)} %collective-permute-done.5.kv_ref), channel_id=1, source_target_pairs={{0,224},{1,225},{2,226},{3,227},{4,228},{5,229},{6,230},{7,231},{8... | collective-permute-start | bytes 1572872 | tf_op jit(solution)/shard_map/ppermute | solution.py:109
  44.2 3.3 %shard_map.73 = (f32[136,1024]{1,0:T(8,128)S(1)}, f32[136,1024]{1,0:T(8,128)S(1)}) custom-call(bf16[128,2048]{1,0:T(8,128)(2,1)S(1)} %maximum_maximum_fusion.q_ref, bf16[1024,256]{1,0:T(8,128)(2,1)S(1)} %bitcast.49), custom_call_target="tpu_custom_call" | custom-call | flops 1073741824 | bytes 8192 | tf_op jit(solution)/shard_map/pallas_call | solution.py:84
  47.4 3.3 %shard_map.74 = (f32[136,1024]{1,0:T(8,128)S(1)}, f32[136,1024]{1,0:T(8,128)S(1)}) custom-call(bf16[128,2048]{1,0:T(8,128)(2,1)S(1)} %maximum_maximum_fusion.q_ref, bf16[1024,256]{1,0:T(8,128)(2,1)S(1)} %collective-permute-done.7.kv_ref, f32[136,1024]{1,0:T(8,128)S(1)} %get-tuple-element.41.refs_0_, ...), custom_call_target="tpu_custom_call", output_to_operand_aliasing={{0}: (2, {}), {1}: (3, {})} | custom-call | flops 1073741824 | bytes 8192 | tf_op jit(solution)/shard_map/pallas_call | solution.py:84
  50.7 3.3 %shard_map.75 = (f32[136,1024]{1,0:T(8,128)S(1)}, f32[136,1024]{1,0:T(8,128)S(1)}) custom-call(bf16[128,2048]{1,0:T(8,128)(2,1)S(1)} %maximum_maximum_fusion.q_ref, bf16[1024,256]{1,0:T(8,128)(2,1)S(1)} %collective-permute-done.5.kv_ref, f32[136,1024]{1,0:T(8,128)S(1)} %get-tuple-element.43.refs_0_, ...), custom_call_target="tpu_custom_call", output_to_operand_aliasing={{0}: (2, {}), {1}: (3, {})} | custom-call | flops 1073741824 | bytes 8192 | tf_op jit(solution)/shard_map/pallas_call | solution.py:84
  54.2 3.3 %shard_map.76 = (f32[136,1024]{1,0:T(8,128)S(1)}, f32[136,1024]{1,0:T(8,128)S(1)}) custom-call(bf16[128,2048]{1,0:T(8,128)(2,1)S(1)} %maximum_maximum_fusion.q_ref, bf16[1024,256]{1,0:T(8,128)(2,1)S(1)} %collective-permute-done.8.kv_ref, f32[136,1024]{1,0:T(8,128)S(1)} %get-tuple-element.48.refs_0_, ...), custom_call_target="tpu_custom_call", output_to_operand_aliasing={{0}: (2, {}), {1}: (3, {})} | custom-call | flops 1073741824 | bytes 8192 | tf_op jit(solution)/shard_map/pallas_call | solution.py:84
  57.5 2.7 %collective-permute-start.9 = (bf16[1024,256]{1,0:T(8,128)(2,1)S(1)}, bf16[1024,256]{1,0:T(8,128)(2,1)S(1)}, u32[]{:S(2)}, u32[]{:S(2)}) collective-permute-start(bf16[1024,256]{1,0:T(8,128)(2,1)S(1)} %collective-permute-done.6.kv_ref), channel_id=1, source_target_pairs={{0,224},{1,225},{2,226},{3,227},{4,228},{5,229},{6,230},{7,231},{8... | collective-permute-start | bytes 1572872 | tf_op jit(solution)/shard_map/ppermute | solution.py:109
  60.2 3.3 %shard_map.77 = (f32[136,1024]{1,0:T(8,128)S(1)}, f32[136,1024]{1,0:T(8,128)S(1)}) custom-call(bf16[128,2048]{1,0:T(8,128)(2,1)S(1)} %maximum_maximum_fusion.q_ref, bf16[1024,256]{1,0:T(8,128)(2,1)S(1)} %collective-permute-done.6.kv_ref, f32[136,1024]{1,0:T(8,128)S(1)} %get-tuple-element.53.refs_0_, ...), custom_call_target="tpu_custom_call", output_to_operand_aliasing={{0}: (2, {}), {1}: (3, {})} | custom-call | flops 1073741824 | bytes 8192 | tf_op jit(solution)/shard_map/pallas_call | solution.py:84
  63.5 1.9 %collective-permute-done.10.kv_ref = bf16[1024,256]{1,0:T(8,128)(2,1)S(1)} collective-permute-done((bf16[1024,256]{1,0:T(8,128)(2,1)S(1)}, bf16[1024,256]{1,0:T(8,128)(2,1)S(1)}, u32[]{:S(2)}, u32[]{:S(2)}) %collective-permute-start.10) | collective-permute-done | bytes 524320 | tf_op jit(solution)/shard_map/ppermute | solution.py:109
  65.5 3.3 %shard_map.78 = (f32[136,1024]{1,0:T(8,128)S(1)}, f32[136,1024]{1,0:T(8,128)S(1)}) custom-call(bf16[128,2048]{1,0:T(8,128)(2,1)S(1)} %maximum_maximum_fusion.q_ref, bf16[1024,256]{1,0:T(8,128)(2,1)S(1)} %collective-permute-done.10.kv_ref, f32[136,1024]{1,0:T(8,128)S(1)} %get-tuple-element.58.refs_0_, ...), custom_call_target="tpu_custom_call", output_to_operand_aliasing={{0}: (2, {}), {1}: (3, {})} | custom-call | flops 1073741824 | bytes 8192 | tf_op jit(solution)/shard_map/pallas_call | solution.py:84
  68.9 3.0 %collective-permute-start.11 = (bf16[512,256]{1,0:T(8,128)(2,1)S(1)}, bf16[512,256]{1,0:T(8,128)(2,1)S(1)}, u32[]{:S(2)}, u32[]{:S(2)}) collective-permute-start(bf16[512,256]{1,0:T(8,128)(2,1)S(1)} %slice.72), channel_id=1, source_target_pairs={{0,224},{1,225},{2,226},{3,227},{4,228},{5,229},{6,230},{7,231},{8... | collective-permute-start | bytes 786440 | tf_op jit(solution)/shard_map/ppermute | solution.py:109
  71.9 3.3 %shard_map.79 = (f32[136,1024]{1,0:T(8,128)S(1)}, f32[136,1024]{1,0:T(8,128)S(1)}) custom-call(bf16[128,2048]{1,0:T(8,128)(2,1)S(1)} %maximum_maximum_fusion.q_ref, bf16[1024,256]{1,0:T(8,128)(2,1)S(1)} %collective-permute-done.9.kv_ref, f32[136,1024]{1,0:T(8,128)S(1)} %get-tuple-element.63.refs_0_, ...), custom_call_target="tpu_custom_call", output_to_operand_aliasing={{0}: (2, {}), {1}: (3, {})} | custom-call | flops 1073741824 | bytes 8192 | tf_op jit(solution)/shard_map/pallas_call | solution.py:84
  75.2 1.6 %shard_map.80 = (f32[136,1024]{1,0:T(8,128)S(1)}, f32[136,1024]{1,0:T(8,128)S(1)}) custom-call(bf16[128,2048]{1,0:T(8,128)(2,1)S(1)} %maximum_maximum_fusion.q_ref, bf16[512,256]{1,0:T(8,128)(2,1)S(1)} %collective-permute-done.12.kv_ref, f32[136,1024]{1,0:T(8,128)S(1)} %get-tuple-element.68.refs_0_, ...), custom_call_target="tpu_custom_call", output_to_operand_aliasing={{0}: (2, {}), {1}: (3, {})} | custom-call | flops 536870912 | bytes 4096 | tf_op jit(solution)/shard_map/pallas_call | solution.py:84
  76.8 1.6 %shard_map.81 = (f32[136,1024]{1,0:T(8,128)S(1)}, f32[136,1024]{1,0:T(8,128)S(1)}) custom-call(bf16[128,2048]{1,0:T(8,128)(2,1)S(1)} %maximum_maximum_fusion.q_ref, bf16[512,256]{1,0:T(8,128)(2,1)S(1)} %collective-permute-done.11.kv_ref, f32[136,1024]{1,0:T(8,128)S(1)} %get-tuple-element.73.refs_0_, ...), custom_call_target="tpu_custom_call", output_to_operand_aliasing={{0}: (2, {}), {1}: (3, {})} | custom-call | flops 536870912 | bytes 4096 | tf_op jit(solution)/shard_map/pallas_call | solution.py:84
  78.4 5.0 %collective-permute-start.13 = (f32[136,1024]{1,0:T(8,128)S(1)}, f32[136,1024]{1,0:T(8,128)S(1)}, u32[]{:S(2)}, u32[]{:S(2)}) collective-permute-start(f32[136,1024]{1,0:T(8,128)S(1)} %get-tuple-element.76), channel_id=1, source_target_pairs={{0,1},{1,0},{2,3},{3,2},{4,5},{5,4},{6,7},{7,6},{8,9},{9,8},{10,11... | collective-permute-start | bytes 1671176 | tf_op jit(solution)/shard_map/ppermute | solution.py:109
  85.3 9.9 %all_to_all.24 = bf16[8,64,128]{2,1,0:T(8,128)(2,1)S(1)} all-to-all(bf16[8,64,128]{2,1,0:T(8,128)(2,1)S(1)} %bitcast.50), channel_id=1, replica_groups=mesh['sp'=32,'tp'=8] {'tp'}, dimensions={0} | all-to-all | bytes 262144 | tf_op jit(solution)/shard_map/all_to_all | solution.py:228
  95.2 1.5 %convolution_convert_fusion = bf16[64,2048]{1,0:T(8,128)(2,1)} fusion(bf16[1024,2048]{1,0:T(8,128)(2,1)S(1)} %copy-done.1, bf16[8,64,128]{2,1,0:T(8,128)(2,1)S(1)} %all_to_all.24), kind=kOutput, calls=%fused_computation | convolution fusion | flops 268566528 | bytes 4587520 | tf_op jit(solution)/shard_map/dot_general | solution.py:229
  (71 shorter events, 9.5 us)
Async XLA Ops:
  0.0 15.9 %copy-start.2 = (bf16[2048,128]{1,0:T(8,128)(2,1)S(1)}, bf16[2048,128]{1,0:T(8,128)(2,1)}, u32[]{:S(2)}) copy-start(bf16[2048,128]{1,0:T(8,128)(2,1)} %param.8) | copy-start | bytes 1572868
  0.0 16.4 %collective-permute-start.1 = (bf16[64,2048]{1,0:T(8,128)(2,1)}, bf16[64,2048]{1,0:T(8,128)(2,1)}, u32[]{:S(2)}, u32[]{:S(2)}) collective-permute-start(bf16[64,2048]{1,0:T(8,128)(2,1)} %param.7), channel_id=1, source_target_pairs={{0,6},{1,7},{2,0},{3,1},{4,2},{5,3},{6,4},{7,5},{8,14},{9,15},{10,... | collective-permute-start | bytes 786440 | tf_op jit(solution)/shard_map/ppermute | solution.py:109
  3.6 14.1 %collective-permute-start.2 = (bf16[64,2048]{1,0:T(8,128)(2,1)}, bf16[64,2048]{1,0:T(8,128)(2,1)S(1)}, u32[]{:S(2)}, u32[]{:S(2)}) collective-permute-start(bf16[64,2048]{1,0:T(8,128)(2,1)} %param.7), channel_id=1, source_target_pairs={{0,4},{1,5},{2,6},{3,7},{4,0},{5,1},{6,2},{7,3},{8,12},{9,13},{10,... | collective-permute-start | bytes 786440 | tf_op jit(solution)/shard_map/ppermute | solution.py:109
  3.9 15.2 %collective-permute-start.3 = (bf16[64,2048]{1,0:T(8,128)(2,1)}, bf16[64,2048]{1,0:T(8,128)(2,1)S(1)}, u32[]{:S(2)}, u32[]{:S(2)}) collective-permute-start(bf16[64,2048]{1,0:T(8,128)(2,1)} %param.7), channel_id=1, source_target_pairs={{0,2},{1,3},{2,4},{3,5},{4,6},{5,7},{6,0},{7,1},{8,10},{9,11},{10,... | collective-permute-start | bytes 786440 | tf_op jit(solution)/shard_map/ppermute | solution.py:109
  4.6 11.6 %collective-permute-start = (bf16[2048,128]{1,0:T(8,128)(2,1)}, bf16[2048,128]{1,0:T(8,128)(2,1)S(1)}, u32[]{:S(2)}, u32[]{:S(2)}) collective-permute-start(bf16[2048,128]{1,0:T(8,128)(2,1)} %param.8), channel_id=1, source_target_pairs={{0,1},{1,0},{2,3},{3,2},{4,5},{5,4},{6,7},{7,6},{8,9},{9,8},{10,11... | collective-permute-start | bytes 1572872 | tf_op jit(solution)/shard_map/ppermute | solution.py:109
  9.0 10.4 %copy-start.3 = (bf16[64,2048]{1,0:T(8,128)(2,1)S(1)}, bf16[64,2048]{1,0:T(8,128)(2,1)}, u32[]{:S(2)}) copy-start(bf16[64,2048]{1,0:T(8,128)(2,1)} %param.7) | copy-start | bytes 786436
  9.9 16.0 %all-to-all-start = ((bf16[16,64,256]{2,1,0:T(8,128)(2,1)}), bf16[16,64,256]{2,1,0:T(8,128)(2,1)S(1)}, u32[]{:S(2)}, u32[]{:S(2)}) async-start(bf16[16,64,256]{2,1,0:T(8,128)(2,1)} %bitcast.14), calls=%async_computation | async-start | bytes 1048576 | tf_op jit(solution)/shard_map/all_to_all | solution.py:168
  20.1 11.7 %collective-permute-start.4 = (bf16[256,256]{1,0:T(8,128)(2,1)S(1)}, bf16[256,256]{1,0:T(8,128)(2,1)S(1)}, u32[]{:S(2)}, u32[]{:S(2)}) collective-permute-start(bf16[256,256]{1,0:T(8,128)(2,1)S(1)} %copy.32), channel_id=1, source_target_pairs={{0,1},{1,0},{2,3},{3,2},{4,5},{5,4},{6,7},{7,6},{8,9},{9,8},{10,11... | collective-permute-start | bytes 393224 | tf_op jit(solution)/shard_map/ppermute | solution.py:109
  25.9 15.6 %collective-permute-start.7 = (bf16[1024,256]{1,0:T(8,128)(2,1)S(1)}, bf16[1024,256]{1,0:T(8,128)(2,1)S(1)}, u32[]{:S(2)}, u32[]{:S(2)}) collective-permute-start(bf16[1024,256]{1,0:T(8,128)(2,1)S(1)} %bitcast.47), channel_id=1, source_target_pairs={{0,32},{1,33},{2,34},{3,35},{4,36},{5,37},{6,38},{7,39},{8,40},{9,... | collective-permute-start | bytes 1572872 | tf_op jit(solution)/shard_map/ppermute | solution.py:109
  27.5 13.9 %collective-permute-start.5 = (bf16[1024,256]{1,0:T(8,128)(2,1)S(1)}, bf16[1024,256]{1,0:T(8,128)(2,1)S(1)}, u32[]{:S(2)}, u32[]{:S(2)}) collective-permute-start(bf16[1024,256]{1,0:T(8,128)(2,1)S(1)} %bitcast.48), channel_id=1, source_target_pairs={{0,224},{1,225},{2,226},{3,227},{4,228},{5,229},{6,230},{7,231},{8... | collective-permute-start | bytes 1572872 | tf_op jit(solution)/shard_map/ppermute | solution.py:109
  41.4 12.6 %collective-permute-start.8 = (bf16[1024,256]{1,0:T(8,128)(2,1)S(1)}, bf16[1024,256]{1,0:T(8,128)(2,1)S(1)}, u32[]{:S(2)}, u32[]{:S(2)}) collective-permute-start(bf16[1024,256]{1,0:T(8,128)(2,1)S(1)} %collective-permute-done.7.kv_ref), channel_id=1, source_target_pairs={{0,32},{1,33},{2,34},{3,35},{4,36},{5,37},{6,38},{7,39},{8,40},{9,... | collective-permute-start | bytes 1572872 | tf_op jit(solution)/shard_map/ppermute | solution.py:109
  41.4 16.0 %collective-permute-start.6 = (bf16[1024,256]{1,0:T(8,128)(2,1)S(1)}, bf16[1024,256]{1,0:T(8,128)(2,1)S(1)}, u32[]{:S(2)}, u32[]{:S(2)}) collective-permute-start(bf16[1024,256]{1,0:T(8,128)(2,1)S(1)} %collective-permute-done.5.kv_ref), channel_id=1, source_target_pairs={{0,224},{1,225},{2,226},{3,227},{4,228},{5,229},{6,230},{7,231},{8... | collective-permute-start | bytes 1572872 | tf_op jit(solution)/shard_map/ppermute | solution.py:109
  54.1 11.3 %collective-permute-start.10 = (bf16[1024,256]{1,0:T(8,128)(2,1)S(1)}, bf16[1024,256]{1,0:T(8,128)(2,1)S(1)}, u32[]{:S(2)}, u32[]{:S(2)}) collective-permute-start(bf16[1024,256]{1,0:T(8,128)(2,1)S(1)} %collective-permute-done.8.kv_ref), channel_id=1, source_target_pairs={{0,32},{1,33},{2,34},{3,35},{4,36},{5,37},{6,38},{7,39},{8,40},{9,... | collective-permute-start | bytes 1572872 | tf_op jit(solution)/shard_map/ppermute | solution.py:109
  57.5 11.3 %collective-permute-start.9 = (bf16[1024,256]{1,0:T(8,128)(2,1)S(1)}, bf16[1024,256]{1,0:T(8,128)(2,1)S(1)}, u32[]{:S(2)}, u32[]{:S(2)}) collective-permute-start(bf16[1024,256]{1,0:T(8,128)(2,1)S(1)} %collective-permute-done.6.kv_ref), channel_id=1, source_target_pairs={{0,224},{1,225},{2,226},{3,227},{4,228},{5,229},{6,230},{7,231},{8... | collective-permute-start | bytes 1572872 | tf_op jit(solution)/shard_map/ppermute | solution.py:109
  65.4 9.7 %collective-permute-start.12 = (bf16[512,256]{1,0:T(8,128)(2,1)S(1)}, bf16[512,256]{1,0:T(8,128)(2,1)S(1)}, u32[]{:S(2)}, u32[]{:S(2)}) collective-permute-start(bf16[512,256]{1,0:T(8,128)(2,1)S(1)} %slice.73), channel_id=1, source_target_pairs={{0,32},{1,33},{2,34},{3,35},{4,36},{5,37},{6,38},{7,39},{8,40},{9,... | collective-permute-start | bytes 786440 | tf_op jit(solution)/shard_map/ppermute | solution.py:109
  68.8 16.1 %copy-start = (f32[128]{0:T(128)S(1)}, f32[128]{0:T(128)}, u32[]{:S(2)}) copy-start(f32[128]{0:T(128)} %param.12) | copy-start | bytes 1540
  68.9 26.3 %copy-start.1 = (bf16[1024,2048]{1,0:T(8,128)(2,1)S(1)}, bf16[1024,2048]{1,0:T(8,128)(2,1)}, u32[]{:S(2)}) copy-start(bf16[1024,2048]{1,0:T(8,128)(2,1)} %param.11) | copy-start | bytes 12582916
  68.9 7.9 %collective-permute-start.11 = (bf16[512,256]{1,0:T(8,128)(2,1)S(1)}, bf16[512,256]{1,0:T(8,128)(2,1)S(1)}, u32[]{:S(2)}, u32[]{:S(2)}) collective-permute-start(bf16[512,256]{1,0:T(8,128)(2,1)S(1)} %slice.72), channel_id=1, source_target_pairs={{0,224},{1,225},{2,226},{3,227},{4,228},{5,229},{6,230},{7,231},{8... | collective-permute-start | bytes 786440 | tf_op jit(solution)/shard_map/ppermute | solution.py:109
  78.4 6.5 %collective-permute-start.13 = (f32[136,1024]{1,0:T(8,128)S(1)}, f32[136,1024]{1,0:T(8,128)S(1)}, u32[]{:S(2)}, u32[]{:S(2)}) collective-permute-start(f32[136,1024]{1,0:T(8,128)S(1)} %get-tuple-element.76), channel_id=1, source_target_pairs={{0,1},{1,0},{2,3},{3,2},{4,5},{5,4},{6,7},{7,6},{8,9},{9,8},{10,11... | collective-permute-start | bytes 1671176 | tf_op jit(solution)/shard_map/ppermute | solution.py:109
